TPU v7x, 32 devices: a whole 2x2x4 slice. The times are simulated.
32 devices in a mesh: fs: 16 (over z, y, x), tp: 2 (over core).
Axes of the slice: x: 2, y: 2, z: 4, core: 2. Of those that a mesh axis runs over, the one named last changes fastest.
Arguments:
- tokens: bfloat16 [4096, 2048], P('fs'), may hold values from -6 to 6
- mix_gain: float32 [2048], replicated, may hold values from 0.1 to 1.9
- glu_value: bfloat16 [2048, 2048], P('fs', 'tp'), may hold values from -0.125 to 0.125
- glu_gate: bfloat16 [2048, 2048], P('fs', 'tp'), may hold values from -0.125 to 0.125
- conv_taps: float32 [31, 2048], P(None, 'tp'), may hold values from -2.2 to 2.2, as said below
- chan_gain: float32 [2048], P('tp'), may hold values from 0.1 to 1.9
- mix_out: bfloat16 [2048, 2048], P('tp', 'fs'), may hold values from -0.125 to 0.125
- mlp_gain: float32 [2048], replicated, may hold values from 0.1 to 1.9
- up_weight: bfloat16 [2048, 8192], P('fs', 'tp'), may hold values from -0.125 to 0.125
- down_weight: bfloat16 [8192, 2048], P('tp', 'fs'), may hold values from -0.0625 to 0.0625
Outputs:
- result: bfloat16 [4096, 2048], P('fs')
Inputs may be any that keep to these rules, and one draw needn't show every extreme that they name: `conv_taps`: independent entries scaled by fan-in; channels fall into 16 groups of different scale.
All inputs are finite; a program needn't handle non-finite values.
Results may differ from a plain program's by a relative error of at most 0.018.
Values may be sent and summed in bfloat16 or wider, within the bound.
No kernel may reach another device: no remote copies, remote signals or barrier semaphores. Data moves between devices by JAX's collectives and lax.ppermute only.
A program may use at most 128 MiB of HBM per device.

v0:
```python
import jax
import jax.numpy as jnp
from jax import lax
from jax.sharding import PartitionSpec as P

C = 2048
LEN = 128
norm_floor = 0.05


def rms_scale(stream, gain):
    return stream * lax.rsqrt(jnp.mean(stream * stream, axis=-1, keepdims=True) + norm_floor) * gain


def bf16_round(value):
    return lax.optimization_barrier(value.astype(jnp.bfloat16)).astype(jnp.float32)


def depthwise(glu, conv_taps):
    seqs = glu.shape[0] // LEN
    blocks = glu.reshape(seqs, LEN, glu.shape[1]).astype(jnp.float32)
    reach = conv_taps.shape[0] // 2
    padded = jnp.pad(blocks, ((0, 0), (reach, reach), (0, 0)))
    total = jnp.zeros_like(blocks)
    for offset in range(conv_taps.shape[0]):
        total = total + padded[:, offset : offset + LEN] * conv_taps[offset]
    return total.reshape(glu.shape)


def per_device(
    tokens,
    mix_gain,
    glu_value,
    glu_gate,
    conv_taps,
    chan_gain,
    mix_out,
    mlp_gain,
    up_weight,
    down_weight,
):
    stream = tokens.astype(jnp.float32)
    normed = rms_scale(stream, mix_gain).astype(jnp.bfloat16)
    values = jnp.dot(
        normed,
        lax.all_gather(glu_value, "fs", axis=0, tiled=True),
        preferred_element_type=jnp.float32,
    )
    gating = jnp.dot(
        normed,
        lax.all_gather(glu_gate, "fs", axis=0, tiled=True),
        preferred_element_type=jnp.float32,
    )
    glu = (values * jax.nn.sigmoid(gating)).astype(jnp.bfloat16)
    convolved = depthwise(glu, conv_taps)
    sums, squares = lax.psum(
        (jnp.sum(convolved, axis=-1), jnp.sum(convolved * convolved, axis=-1)), "tp"
    )
    centre = (sums / C)[:, None]
    spread = (squares / C)[:, None] - centre * centre
    hidden = jax.nn.silu((convolved - centre) * lax.rsqrt(spread + norm_floor) * chan_gain).astype(
        jnp.bfloat16
    )
    whole_out = lax.all_gather(mix_out, "fs", axis=1, tiled=True)
    own_rows = stream.shape[0] // lax.axis_size("tp")
    mixed = lax.psum_scatter(
        jnp.dot(hidden, whole_out, preferred_element_type=jnp.float32).astype(jnp.bfloat16),
        "tp",
        scatter_dimension=0,
        tiled=True,
    ).astype(jnp.float32)
    own_stream = lax.dynamic_slice_in_dim(stream, lax.axis_index("tp") * own_rows, own_rows, 0)
    resid = own_stream + bf16_round(mixed)
    normed_mlp = rms_scale(resid, mlp_gain).astype(jnp.bfloat16)
    whole_up = lax.all_gather(up_weight, "fs", axis=0, tiled=True)
    active = jnp.square(
        jax.nn.relu(
            jnp.dot(
                lax.all_gather(normed_mlp, "tp", axis=0, tiled=True),
                whole_up,
                preferred_element_type=jnp.float32,
            )
        )
    ).astype(jnp.bfloat16)
    whole_down = lax.all_gather(down_weight, "fs", axis=1, tiled=True)
    feed = lax.psum_scatter(
        jnp.dot(active, whole_down, preferred_element_type=jnp.float32).astype(jnp.bfloat16),
        "tp",
        scatter_dimension=0,
        tiled=True,
    ).astype(jnp.float32)
    finished = (resid + bf16_round(feed)).astype(jnp.bfloat16)
    return lax.all_gather(finished, "tp", axis=0, tiled=True)


def solution(mesh):
    in_specs = (
        P("fs", None),
        P(),
        P("fs", "tp"),
        P("fs", "tp"),
        P(None, "tp"),
        P("tp"),
        P("tp", "fs"),
        P(),
        P("fs", "tp"),
        P("tp", "fs"),
    )
    out_specs = P("fs", None)
    return jax.shard_map(
        per_device, mesh=mesh, in_specs=in_specs, out_specs=out_specs, check_vma=False
    )
```

profile of v0, /device:TPU:0, one launch (start us, length us, event | category | flops | bytes accessed | tf_op | source)
XLA Modules:
  0.0 769.7 jit_solution(15755725362399529471)
XLA Ops:
  6.5 0.0 all-gather.10.cloned.1.call-start
  6.5 0.7 all-gather.10.cloned.1.call-update
  7.3 0.0 all-gather.8.cloned.1.call-start
  7.3 0.7 all-gather.8.cloned.1.call-update
  8.0 0.0 all-gather.12.cloned.1.call-start
  8.1 0.7 all-gather.12.cloned.1.call-update
  8.7 0.0 reduce-scatter.3.cloned.1.call-start
  8.8 1.5 multiply_reduce_fusion
  10.3 1.1 fusion.72
  11.4 1.4 fusion.71
  12.8 0.0 copy-start.1
  12.8 0.0 copy-start.4
  12.9 75.6 %all-gather.10.cloned.1.call-done = bf16[2048,1024]{1,0:T(8,128)(2,1)} async-done(((bf16[128,1024]{1,0:T(8,128)(2,1)}), bf16[2048,1024]{1,0:T(8,128)(2,1)}) %all-gather.10.cloned.1.call-update) | async-done | bytes 4194320 | tf_op jit(solution)/shard_map/all_gather | solution.py:51
  88.4 3.9 fusion.4
  92.4 0.0 copy-start.3
  92.4 73.1 %all-gather.8.cloned.1.call-done = bf16[2048,1024]{1,0:T(8,128)(2,1)} async-done(((bf16[128,1024]{1,0:T(8,128)(2,1)}), bf16[2048,1024]{1,0:T(8,128)(2,1)}) %all-gather.8.cloned.1.call-update) | async-done | bytes 4194320 | tf_op jit(solution)/shard_map/all_gather | solution.py:46
  165.4 0.0 copy-done.1
  165.4 0.0 copy-done.4
  165.4 3.5 bitcast_convert_fusion
  169.0 5.7 fusion.69
  174.7 2.5 all-reduce.1
  177.2 0.0 copy-done.3
  177.2 0.4 multiply_convert_fusion.2
  177.6 77.9 %all-gather.12.cloned.1.call-done = bf16[1024,2048]{1,0:T(8,128)(2,1)} async-done(((bf16[1024,128]{1,0:T(8,128)(2,1)}), bf16[1024,2048]{1,0:T(8,128)(2,1)}) %all-gather.12.cloned.1.call-update) | async-done | bytes 4194320 | tf_op jit(solution)/shard_map/all_gather | solution.py:64
  255.5 4.4 convolution_convert_fusion.1
  259.9 0.0 copy-start.2
  259.9 0.0 reduce-scatter.3.cloned.1.call-update
  259.9 0.0 all-gather.14.cloned.1.call-start
  260.0 0.2 convert_element_type.45
  260.2 6.4 reduce-scatter.3.cloned.1.call-done
  266.7 1.3 multiply_reduce_fusion.1
  267.9 0.0 copy-done.2
  267.9 2.0 multiply_convert_fusion.1
  270.0 0.0 all-gather.14.cloned.1.call-update
  270.0 0.0 all-gather.16.cloned.1.call-start
  270.0 0.5 all-gather.16.cloned.1.call-update
  270.6 0.0 all-gather.18.cloned.1.call-start
  270.6 0.7 all-gather.18.cloned.1.call-update
  271.3 0.0 copy-start
  271.3 0.0 reduce-scatter.5.cloned.1.call-start
  271.4 9.0 %all-gather.14.cloned.1.call-done = bf16[256,2048]{1,0:T(8,128)(2,1)} async-done(((bf16[128,2048]{1,0:T(8,128)(2,1)}), bf16[256,2048]{1,0:T(8,128)(2,1)}) %all-gather.14.cloned.1.call-update) | async-done | bytes 1048592 | tf_op jit(solution)/shard_map/all_gather | solution.py:79
  280.4 194.8 %all-gather.16.cloned.1.call-done = bf16[2048,4096]{1,0:T(8,128)(2,1)} async-done(((bf16[128,4096]{1,0:T(8,128)(2,1)}), bf16[2048,4096]{1,0:T(8,128)(2,1)}) %all-gather.16.cloned.1.call-update) | async-done | bytes 16777232 | tf_op jit(solution)/shard_map/all_gather | solution.py:75
  475.2 250.0 %all-gather.18.cloned.1.call-done = bf16[4096,2048]{1,0:T(8,128)(2,1)} async-done(((bf16[4096,128]{1,0:T(8,128)(2,1)}), bf16[4096,2048]{1,0:T(8,128)(2,1)}) %all-gather.18.cloned.1.call-update) | async-done | bytes 16777232 | tf_op jit(solution)/shard_map/all_gather | solution.py:85
  725.2 16.4 %convolution_convert_fusion = bf16[256,2048]{1,0:T(8,128)(2,1)} fusion(bf16[4096,2048]{1,0:T(8,128)(2,1)} %all-gather.18.cloned.1.call-done, bf16[256,2048]{1,0:T(8,128)(2,1)} %all-gather.14.cloned.1.call-done, bf16[2048,4096]{1,0:T(8,128)(2,1)} %all-gather.16.cloned.1.call-done), kind=kOutput, calls=%fused_computation.33 | convolution fusion | flops 8593604608 | bytes 35651584 | tf_op jit(solution)/shard_map/dot_general | solution.py:87
  741.7 0.0 reduce-scatter.5.cloned.1.call-update
  741.7 0.0 all-gather.20.cloned.1.call-start
  741.8 6.7 reduce-scatter.5.cloned.1.call-done
  748.4 0.0 copy-done
  748.4 2.0 add_convert_fusion
  750.5 0.0 all-gather.20.cloned.1.call-update
  750.5 10.4 %all-gather.20.cloned.1.call-done = bf16[256,2048]{1,0:T(8,128)(2,1)} async-done(((bf16[128,2048]{1,0:T(8,128)(2,1)}), bf16[256,2048]{1,0:T(8,128)(2,1)}) %all-gather.20.cloned.1.call-update) | async-done | bytes 1048592 | tf_op jit(solution)/shard_map/all_gather | solution.py:93
  760.9 2.3 copy.12
  (3 shorter events, 0.0 us)
Async XLA Ops:
  6.5 81.9 %all-gather.10.cloned.1.call-start = ((), (), s32[]{:S(2)}) async-start(), calls=%async_computation.3 | async-start | bytes 4456448 | tf_op jit(solution)/shard_map/all_gather | solution.py:51
  7.3 158.2 %all-gather.8.cloned.1.call-start = ((), (), s32[]{:S(2)}) async-start(), calls=%async_computation.2 | async-start | bytes 4456448 | tf_op jit(solution)/shard_map/all_gather | solution.py:46
  8.0 247.5 %all-gather.12.cloned.1.call-start = ((), (), s32[]{:S(2)}) async-start(), calls=%async_computation.4 | async-start | bytes 4456448 | tf_op jit(solution)/shard_map/all_gather | solution.py:64
  8.7 257.9 %reduce-scatter.3.cloned.1.call-start = ((), (), s32[]{:S(2)}) async-start(), calls=%async_computation.5 | async-start | bytes 1572864 | tf_op jit(solution)/shard_map/reduce_scatter | solution.py:66
  12.8 152.6 %copy-start.1 = (bf16[256,2048]{1,0:T(8,128)(2,1)S(1)}, bf16[256,2048]{1,0:T(8,128)(2,1)}, u32[]{:S(2)}) copy-start(bf16[256,2048]{1,0:T(8,128)(2,1)} %param.10) | copy-start | bytes 3145732
  12.8 152.6 %copy-start.4 = (f32[2048]{0:T(1024)S(1)}, f32[2048]{0:T(1024)}, u32[]{:S(2)}) copy-start(f32[2048]{0:T(1024)} %param.11) | copy-start | bytes 24580
  92.4 84.8 %copy-start.3 = (f32[1024]{0:T(1024)S(1)}, f32[1024]{0:T(1024)}, u32[]{:S(2)}) copy-start(f32[1024]{0:T(1024)} %param.15) | copy-start | bytes 12292
  259.9 8.0 %copy-start.2 = (f32[2048]{0:T(1024)S(1)}, f32[2048]{0:T(1024)}, u32[]{:S(2)}) copy-start(f32[2048]{0:T(1024)} %param.17) | copy-start | bytes 24580
  259.9 20.4 %all-gather.14.cloned.1.call-start = ((), (), s32[]{:S(2)}) async-start(), calls=%async_computation.6 | async-start | bytes 1572864 | tf_op jit(solution)/shard_map/all_gather | solution.py:79
  270.0 205.2 %all-gather.16.cloned.1.call-start = ((), (), s32[]{:S(2)}) async-start(), calls=%async_computation.7 | async-start | bytes 17825792 | tf_op jit(solution)/shard_map/all_gather | solution.py:75
  270.6 454.7 %all-gather.18.cloned.1.call-start = ((), (), s32[]{:S(2)}) async-start(), calls=%async_computation.8 | async-start | bytes 17825792 | tf_op jit(solution)/shard_map/all_gather | solution.py:85
  271.3 477.1 %copy-start = (bf16[128,2048]{1,0:T(8,128)(2,1)S(1)}, bf16[128,2048]{1,0:T(8,128)(2,1)}, u32[]{:S(2)}) copy-start(bf16[128,2048]{1,0:T(8,128)(2,1)} %reduce-scatter.3.cloned.1.call-done) | copy-start | bytes 1572868
  271.3 477.1 %reduce-scatter.5.cloned.1.call-start = ((), (), s32[]{:S(2)}) async-start(), calls=%async_computation.9 | async-start | bytes 1572864 | tf_op jit(solution)/shard_map/reduce_scatter | solution.py:86
  741.7 19.2 %all-gather.20.cloned.1.call-start = ((), (), s32[]{:S(2)}) async-start(), calls=%async_computation.10 | async-start | bytes 1572864 | tf_op jit(solution)/shard_map/all_gather | solution.py:93
Sparse Core Ops, SparseCore 0:
  10.1 78.3 all-gather.9
  91.2 74.1 all-gather.7
  168.1 87.3 all-gather.11
  260.1 6.5 reduce-scatter.2
  270.1 10.2 all-gather.13
  283.0 192.1 all-gather.15
  477.9 247.2 all-gather.17
  741.8 6.5 reduce-scatter.4
  750.6 10.2 all-gather.19
where the time goes:
time: 770 us
  waiting for transfers between devices  707 us (92%)
  matrix products  28.3 us (4%)
  between operations  13.3 us (2%)
  other arithmetic  13.2 us (2%)
    all_gather x1, waiting for transfers between devices, per_device(): whole_down = lax.all_gather(down_weight, 'fs', axis=1, tiled=True)  250 us
    all_gather x1, waiting for transfers between devices, per_device(): whole_up = lax.all_gather(up_weight, 'fs', axis=0, tiled=True)  195 us
    all_gather x1, waiting for transfers between devices, per_device(): whole_out = lax.all_gather(mix_out, 'fs', axis=1, tiled=True)  77.9 us
    all_gather x1, waiting for transfers between devices, per_device(): lax.all_gather(glu_gate, 'fs', axis=0, tiled=True)  75.6 us
    all_gather x1, waiting for transfers between devices, per_device(): lax.all_gather(glu_value, 'fs', axis=0, tiled=True)  73.1 us
    dot_general x1, matrix products, per_device(): jnp.dot(active, whole_down, preferred_element_type=jnp.float32)  16.4 us
  transfers between devices with their start and end apart: 9, of which 9 were waited for; matrix products, arithmetic and copies ran while one was open for 2% of the time, Pallas kernels for 0%

commit v1 on v0

--- a/solution.py
+++ b/solution.py
@@ -82,7 +82,8 @@
             )
         )
     ).astype(jnp.bfloat16)
-    whole_down = lax.all_gather(down_weight, "fs", axis=1, tiled=True)
+    pieces = lax.all_gather(down_weight, "fs", axis=0, tiled=False)
+    whole_down = jnp.concatenate(pieces, axis=1)
     feed = lax.psum_scatter(
         jnp.dot(active, whole_down, preferred_element_type=jnp.float32).astype(jnp.bfloat16),
         "tp",

time: 770 us -> 711 us (0.923)
  waiting for transfers between devices: 707 us -> 626 us
  local copies, waits for them, and re-layouts: 4.85 us -> 25.6 us
    all_gather x1, waiting for transfers between devices: 250 us -> 191 us  [per_device(): pieces = lax.all_gather(down_weight, 'fs', axis=0, tiled=False)]
    reshape x0 -> x1, local copies, waits for them, and re-layouts: none -> 20.8 us  [per_device(): whole_down = jnp.concatenate(pieces, axis=1)]
    all_gather x1, waiting for transfers between devices: 195 us -> 183 us  [per_device(): whole_up = lax.all_gather(up_weight, 'fs', axis=0, tiled=True)]
    all_gather x1, waiting for transfers between devices: 9.01 us -> 0.01 us  [per_device(): lax.all_gather(normed_mlp, 'tp', axis=0, tiled=True)]
  transfers between devices with their start and end apart: 9 -> 9, of which waited for: 9 -> 8; matrix products, arithmetic and copies ran while one was open for 2% -> 6% of each run, Pallas kernels for 0% -> 0%
where the time goes in v1:
time: 711 us; the launch traced here: 710 us
  waiting for transfers between devices  626 us (88%)
  matrix products  28.3 us (4%)
  local copies, waits for them, and re-layouts  25.6 us (4%)
  between operations  13.3 us (2%)
  other arithmetic  13.2 us (2%)
    all_gather x1, waiting for transfers between devices, per_device(): pieces = lax.all_gather(down_weight, 'fs', axis=0, tiled=False)  191 us
    all_gather x1, waiting for transfers between devices, per_device(): whole_up = lax.all_gather(up_weight, 'fs', axis=0, tiled=True)  183 us
    all_gather x1, waiting for transfers between devices, per_device(): whole_out = lax.all_gather(mix_out, 'fs', axis=1, tiled=True)  77.9 us
    all_gather x1, waiting for transfers between devices, per_device(): lax.all_gather(glu_gate, 'fs', axis=0, tiled=True)  75.6 us
    all_gather x1, waiting for transfers between devices, per_device(): lax.all_gather(glu_value, 'fs', axis=0, tiled=True)  73.1 us
    reshape x1, local copies, waits for them, and re-layouts, per_device(): whole_down = jnp.concatenate(pieces, axis=1)  20.8 us
    dot_general x1, matrix products, per_device(): jnp.dot(active, whole_down, preferred_element_type=jnp.float32)  16.5 us
  transfers between devices with their start and end apart: 9, of which 8 were waited for; matrix products, arithmetic and copies ran while one was open for 6% of the time, Pallas kernels for 0%

profile of v1, /device:TPU:0, one launch (start us, length us, event | category | flops | bytes accessed | tf_op | source)
XLA Modules:
  0.0 709.7 jit_solution(16312465658057118294)
XLA Ops:
  6.5 0.0 all-gather.11.cloned.1.call-start
  6.5 0.7 all-gather.11.cloned.1.call-update
  7.3 0.0 all-gather.9.cloned.1.call-start
  7.3 0.7 all-gather.9.cloned.1.call-update
  8.0 0.0 all-gather.13.cloned.1.call-start
  8.1 0.7 all-gather.13.cloned.1.call-update
  8.7 0.0 reduce-scatter.3.cloned.1.call-start
  8.8 1.5 multiply_reduce_fusion
  10.3 1.1 fusion.72
  11.4 1.4 fusion.71
  12.8 0.0 copy-start.1
  12.8 0.0 copy-start.4
  12.8 75.6 %all-gather.11.cloned.1.call-done = bf16[2048,1024]{1,0:T(8,128)(2,1)} async-done(((bf16[128,1024]{1,0:T(8,128)(2,1)}), bf16[2048,1024]{1,0:T(8,128)(2,1)}) %all-gather.11.cloned.1.call-update) | async-done | bytes 4194320 | tf_op jit(solution)/shard_map/all_gather | solution.py:51
  88.4 3.9 fusion.4
  92.4 0.0 copy-start.3
  92.4 73.1 %all-gather.9.cloned.1.call-done = bf16[2048,1024]{1,0:T(8,128)(2,1)} async-done(((bf16[128,1024]{1,0:T(8,128)(2,1)}), bf16[2048,1024]{1,0:T(8,128)(2,1)}) %all-gather.9.cloned.1.call-update) | async-done | bytes 4194320 | tf_op jit(solution)/shard_map/all_gather | solution.py:46
  165.4 0.0 copy-done.1
  165.4 0.0 copy-done.4
  165.4 3.5 bitcast_convert_fusion
  168.9 5.7 fusion.69
  174.6 2.5 all-reduce.1
  177.1 0.0 copy-done.3
  177.1 0.4 multiply_convert_fusion.2
  177.6 77.9 %all-gather.13.cloned.1.call-done = bf16[1024,2048]{1,0:T(8,128)(2,1)} async-done(((bf16[1024,128]{1,0:T(8,128)(2,1)}), bf16[1024,2048]{1,0:T(8,128)(2,1)}) %all-gather.13.cloned.1.call-update) | async-done | bytes 4194320 | tf_op jit(solution)/shard_map/all_gather | solution.py:64
  255.5 4.4 convolution_convert_fusion.1
  259.9 0.0 copy-start.2
  259.9 0.0 reduce-scatter.3.cloned.1.call-update
  259.9 0.0 all-gather.21.cloned.1.call-start
  260.0 0.5 all-gather.21.cloned.1.call-update
  260.5 0.0 all-gather.15.cloned.1.call-start
  260.6 0.2 convert_element_type.45
  260.8 5.8 reduce-scatter.3.cloned.1.call-done
  266.7 1.3 multiply_reduce_fusion.1
  267.9 0.0 copy-done.2
  267.9 2.0 multiply_convert_fusion.1
  270.0 0.0 all-gather.15.cloned.1.call-update
  270.0 0.0 all-gather.17.cloned.1.call-start
  270.0 0.7 all-gather.17.cloned.1.call-update
  270.7 0.2 reduce-scatter.5.cloned.1.call-start
  271.0 190.6 %all-gather.21.cloned.1.call-done = bf16[65536,128]{1,0:T(8,128)(2,1)} async-done(((bf16[4096,128]{1,0:T(8,128)(2,1)}), bf16[65536,128]{1,0:T(8,128)(2,1)}) %all-gather.21.cloned.1.call-update) | async-done | bytes 16777232 | tf_op jit(solution)/shard_map/all_gather | solution.py:85
  461.5 20.8 %copy.11 = bf16[4096,16,128]{0,2,1:T(8,128)(2,1)} copy(bf16[4096,16,128]{2,0,1:T(8,128)(2,1)} %bitcast.57) | data formatting | bytes 33554432 | tf_op jit(solution)/shard_map/reshape | solution.py:86
  482.3 0.0 all-gather.15.cloned.1.call-done
  482.3 182.8 %all-gather.17.cloned.1.call-done = bf16[2048,4096]{1,0:T(8,128)(2,1)} async-done(((bf16[128,4096]{1,0:T(8,128)(2,1)}), bf16[2048,4096]{1,0:T(8,128)(2,1)}) %all-gather.17.cloned.1.call-update) | async-done | bytes 16777232 | tf_op jit(solution)/shard_map/all_gather | solution.py:75
  665.1 0.0 copy-start
  665.1 16.5 %convolution_convert_fusion = bf16[256,2048]{1,0:T(8,128)(2,1)} fusion(bf16[4096,2048]{0,1:T(8,128)(2,1)} %bitcast.58, bf16[256,2048]{1,0:T(8,128)(2,1)} %all-gather.15.cloned.1.call-done, bf16[2048,4096]{1,0:T(8,128)(2,1)} %all-gather.17.cloned.1.call-done), kind=kOutput, calls=%fused_computation.33 | convolution fusion | flops 8593604608 | bytes 35651584 | tf_op jit(solution)/shard_map/dot_general | solution.py:88
  681.7 0.0 reduce-scatter.5.cloned.1.call-update
  681.7 0.0 all-gather.19.cloned.1.call-start
  681.7 6.7 reduce-scatter.5.cloned.1.call-done
  688.4 0.0 copy-done
  688.4 2.0 add_convert_fusion
  690.4 0.0 all-gather.19.cloned.1.call-update
  690.5 10.4 %all-gather.19.cloned.1.call-done = bf16[256,2048]{1,0:T(8,128)(2,1)} async-done(((bf16[128,2048]{1,0:T(8,128)(2,1)}), bf16[256,2048]{1,0:T(8,128)(2,1)}) %all-gather.19.cloned.1.call-update) | async-done | bytes 1048592 | tf_op jit(solution)/shard_map/all_gather | solution.py:94
  700.9 2.3 copy.13
  (3 shorter events, 0.0 us)
Async XLA Ops:
  6.5 81.9 %all-gather.11.cloned.1.call-start = ((), (), s32[]{:S(2)}) async-start(), calls=%async_computation.3 | async-start | bytes 4456448 | tf_op jit(solution)/shard_map/all_gather | solution.py:51
  7.3 158.2 %all-gather.9.cloned.1.call-start = ((), (), s32[]{:S(2)}) async-start(), calls=%async_computation.2 | async-start | bytes 4456448 | tf_op jit(solution)/shard_map/all_gather | solution.py:46
  8.0 247.5 %all-gather.13.cloned.1.call-start = ((), (), s32[]{:S(2)}) async-start(), calls=%async_computation.4 | async-start | bytes 4456448 | tf_op jit(solution)/shard_map/all_gather | solution.py:64
  8.7 257.9 %reduce-scatter.3.cloned.1.call-start = ((), (), s32[]{:S(2)}) async-start(), calls=%async_computation.5 | async-start | bytes 1572864 | tf_op jit(solution)/shard_map/reduce_scatter | solution.py:66
  12.8 152.6 %copy-start.1 = (bf16[256,2048]{1,0:T(8,128)(2,1)S(1)}, bf16[256,2048]{1,0:T(8,128)(2,1)}, u32[]{:S(2)}) copy-start(bf16[256,2048]{1,0:T(8,128)(2,1)} %param.10) | copy-start | bytes 3145732
  12.8 152.6 %copy-start.4 = (f32[2048]{0:T(1024)S(1)}, f32[2048]{0:T(1024)}, u32[]{:S(2)}) copy-start(f32[2048]{0:T(1024)} %param.11) | copy-start | bytes 24580
  92.4 84.8 %copy-start.3 = (f32[1024]{0:T(1024)S(1)}, f32[1024]{0:T(1024)}, u32[]{:S(2)}) copy-start(f32[1024]{0:T(1024)} %param.15) | copy-start | bytes 12292
  259.9 8.0 %copy-start.2 = (f32[2048]{0:T(1024)S(1)}, f32[2048]{0:T(1024)}, u32[]{:S(2)}) copy-start(f32[2048]{0:T(1024)} %param.17) | copy-start | bytes 24580
  259.9 201.6 %all-gather.21.cloned.1.call-start = ((), (), s32[]{:S(2)}) async-start(), calls=%async_computation.10 | async-start | bytes 17825792 | tf_op jit(solution)/shard_map/all_gather | solution.py:85
  260.5 221.8 %all-gather.15.cloned.1.call-start = ((), (), s32[]{:S(2)}) async-start(), calls=%async_computation.6 | async-start | bytes 1572864 | tf_op jit(solution)/shard_map/all_gather | solution.py:79
  270.0 395.2 %all-gather.17.cloned.1.call-start = ((), (), s32[]{:S(2)}) async-start(), calls=%async_computation.7 | async-start | bytes 17825792 | tf_op jit(solution)/shard_map/all_gather | solution.py:75
  270.7 417.7 %reduce-scatter.5.cloned.1.call-start = ((), (), s32[]{:S(2)}) async-start(), calls=%async_computation.8 | async-start | bytes 1572864 | tf_op jit(solution)/shard_map/reduce_scatter | solution.py:87
  665.1 23.3 %copy-start = (bf16[128,2048]{1,0:T(8,128)(2,1)S(1)}, bf16[128,2048]{1,0:T(8,128)(2,1)}, u32[]{:S(2)}) copy-start(bf16[128,2048]{1,0:T(8,128)(2,1)} %reduce-scatter.3.cloned.1.call-done) | copy-start | bytes 1572868
  681.7 19.2 %all-gather.19.cloned.1.call-start = ((), (), s32[]{:S(2)}) async-start(), calls=%async_computation.9 | async-start | bytes 1572864 | tf_op jit(solution)/shard_map/all_gather | solution.py:94
Sparse Core Ops, SparseCore 0:
  10.1 78.3 all-gather.10
  91.2 74.1 all-gather.8
  168.1 87.3 all-gather.12
  260.1 6.5 reduce-scatter.2
  269.3 192.2 all-gather.20
  462.9 7.1 all-gather.14
  472.9 192.1 all-gather.16
  681.8 6.5 reduce-scatter.4
  690.6 10.2 all-gather.18
